TPU v7x, 32 devices: a whole 2x2x4 slice. The times are simulated.
32 devices in a mesh: sp: 16 (over z, y, x), tp: 2 (over core).
Axes of the slice: x: 2, y: 2, z: 4, core: 2. Of those that a mesh axis runs over, the one named last changes fastest.
Arguments:
- query_rows: bfloat16 [4096, 1024], P('sp', 'tp'), may hold values from -6 to 6
- key_rows: bfloat16 [4096, 1024], P('sp', 'tp'), may hold values from -6 to 6
- value_rows: bfloat16 [4096, 1024], P('sp', 'tp'), may hold values from -6 to 6
- out_weight: bfloat16 [1024, 2048], P('tp'), may hold values from -0.75 to 0.75
Outputs:
- layer_out: bfloat16 [4096, 2048], P(('sp', 'tp'))
All inputs are finite; a program needn't handle non-finite values.
Results may differ from a plain program's by a relative error of at most 0.012.
Values may be sent and summed in bfloat16 or wider, within the bound.
A program may use at most 64 MiB of HBM per device.

v0:
```python
import math

import jax
import jax.numpy as jnp
from jax import lax
from jax.sharding import PartitionSpec as P

HD = 64
BACK = 128


THETA = 500000.0
DILATIONS = (1, 4, 16)


def shifted(value, axis, steps):
    count = lax.axis_size(axis)
    initial, last = (max(0, -steps), min(count, count - steps))
    return lax.ppermute(value, axis, [(source, source + steps) for source in range(initial, last)])


def rotate(rows, positions, head_count, head_dim):
    half_dim = head_dim // 2
    inverse = jnp.power(jnp.float32(THETA), -jnp.arange(half_dim, dtype=jnp.float32) / half_dim)
    angles = positions.astype(jnp.float32)[:, None] * inverse[None, :]
    cosine = jnp.cos(angles)[:, None, :]
    sine = jnp.sin(angles)[:, None, :]
    whole = rows.astype(jnp.float32).reshape(rows.shape[0], head_count, head_dim)
    lower = whole[..., :half_dim]
    upper = whole[..., half_dim:]
    turned = jnp.concatenate(
        [lower * cosine - upper * sine, upper * cosine + lower * sine], axis=-1
    )
    return turned.reshape(rows.shape[0], head_count * head_dim).astype(jnp.bfloat16)


def pattern_part(queries, key_ext, value_ext, dilation, anchor, head_count):
    tok_rows = queries.shape[0]
    length = tok_rows // dilation
    nblocks = max(1, length // BACK)
    block_rows = length // nblocks
    query_sub = queries.reshape(length, dilation, head_count, HD)
    key_sub = key_ext.reshape(BACK + length, dilation, head_count, HD)
    value_sub = value_ext.reshape(BACK + length, dilation, head_count, HD)
    residues = jnp.arange(dilation, dtype=jnp.int32)[:, None, None, None]
    results, maxima, sums = ([], [], [])
    for block_index in range(nblocks):
        first_row = block_index * block_rows
        key_part = key_sub[first_row : first_row + BACK + block_rows]
        value_part = value_sub[first_row : first_row + BACK + block_rows]
        scores = jnp.einsum(
            "qrhc,krhc->rhqk",
            query_sub[first_row : first_row + block_rows],
            key_part,
            preferred_element_type=jnp.float32,
        ) * (1.0 / math.sqrt(HD))
        query_index = jnp.arange(block_rows, dtype=jnp.int32)[:, None]
        key_index = jnp.arange(BACK + block_rows, dtype=jnp.int32)[None, :]
        distance = query_index + BACK - key_index
        key_position = anchor + (first_row + key_index - BACK) * dilation + residues
        allowed = (distance >= 0) & (distance <= BACK) & (key_position >= 0)
        scores = jnp.where(allowed, scores, -jnp.inf)
        row_max = jnp.max(scores, axis=-1)
        weights = jnp.exp(scores - row_max[..., None])
        row_sum = jnp.sum(weights, axis=-1)
        weighted = jnp.einsum(
            "rhqk,krhc->qrhc",
            weights.astype(jnp.bfloat16),
            value_part,
            preferred_element_type=jnp.float32,
        )
        sum_rows = row_sum.transpose(2, 0, 1)
        results.append((weighted / sum_rows[..., None]).astype(jnp.bfloat16))
        maxima.append(row_max.transpose(2, 0, 1))
        sums.append(sum_rows)
    result = jnp.concatenate(results, axis=0).reshape(tok_rows, head_count, HD)
    row_max = jnp.concatenate(maxima, axis=0).reshape(tok_rows, head_count)
    row_sum = jnp.concatenate(sums, axis=0).reshape(tok_rows, head_count)
    return (result, row_max, row_sum)


def per_device(query_rows, key_rows, value_rows, out_weight):
    tok_rows = query_rows.shape[0]
    head_count = query_rows.shape[1] // HD
    anchor = lax.axis_index("sp") * tok_rows
    positions = anchor + jnp.arange(tok_rows, dtype=jnp.int32)
    turned_q = rotate(query_rows, positions, head_count, HD)
    turned_k = rotate(key_rows, positions, head_count, HD)
    paired = jnp.stack((turned_k, value_rows))
    pieces = -(-(16 * BACK) // tok_rows)
    held = paired
    gathered = 1
    while gathered < pieces + 1:
        needed = min(gathered, pieces + 1 - gathered)
        arrived = shifted(held[:, held.shape[1] - needed * tok_rows :], "sp", gathered)
        held = jnp.concatenate([arrived, held], axis=1)
        gathered = gathered + needed
    prior = held[:, : held.shape[1] - tok_rows]
    results, maxima, sums = ([], [], [])
    for dilation in DILATIONS:
        reach = BACK * dilation
        key_ext = jnp.concatenate([prior[0, prior.shape[1] - reach :], turned_k], axis=0)
        value_ext = jnp.concatenate([prior[1, prior.shape[1] - reach :], value_rows], axis=0)
        result, row_max, row_sum = pattern_part(
            turned_q, key_ext, value_ext, dilation, anchor, head_count
        )
        results.append(result)
        maxima.append(row_max)
        sums.append(row_sum)
    top = jnp.maximum(jnp.maximum(maxima[0], maxima[1]), maxima[2])
    scales = [sums[i] * jnp.exp(maxima[i] - top) for i in range(3)]
    weighted = scales[0][..., None] * results[0].astype(jnp.float32)
    weighted = weighted + scales[1][..., None] * results[1].astype(jnp.float32)
    weighted = weighted + scales[2][..., None] * results[2].astype(jnp.float32)
    denominator = scales[0] + scales[1] + scales[2]
    mixed = (
        (weighted / denominator[..., None]).reshape(tok_rows, head_count * HD).astype(jnp.bfloat16)
    )
    projected = lax.psum_scatter(
        jnp.dot(mixed, out_weight, preferred_element_type=jnp.float32),
        "tp",
        scatter_dimension=0,
        tiled=True,
    )
    return projected.astype(jnp.bfloat16)


def solution(mesh):
    return jax.shard_map(
        per_device,
        mesh=mesh,
        in_specs=(P("sp", "tp"), P("sp", "tp"), P("sp", "tp"), P("tp", None)),
        out_specs=P(("sp", "tp"), None),
        check_vma=False,
    )
```

profile of v0, /device:TPU:17, one launch (start us, length us, event | category | flops | bytes accessed | tf_op | source)
XLA Modules:
  0.0 220.9 jit_solution(2691751805251715072)
XLA Ops:
  11.0 1.3 collective-permute-start.2
  12.3 3.1 %collective-permute-start = (bf16[2,256,512]{2,1,0:T(8,128)(2,1)}, bf16[2,256,512]{2,1,0:T(8,128)(2,1)S(1)}, u32[]{:S(2)}, u32[]{:S(2)}) collective-permute-start(bf16[2,256,512]{2,1,0:T(8,128)(2,1)} %pad_maximum_fusion.4), channel_id=1, source_target_pairs={{0,2},{2,4},{4,6},{6,8},{8,10},{10,12},{12,14},{14,16},{16,18},{18... | collective-permute-start | bytes 1572872 | tf_op jit(solution)/shard_map/ppermute | solution.py:19
  17.2 2.0 copy.139
  20.0 32.3 %collective-permute-done = bf16[2,256,512]{2,1,0:T(8,128)(2,1)S(1)} collective-permute-done((bf16[2,256,512]{2,1,0:T(8,128)(2,1)}, bf16[2,256,512]{2,1,0:T(8,128)(2,1)S(1)}, u32[]{:S(2)}, u32[]{:S(2)}) %collective-permute-start) | collective-permute-done | bytes 524320 | tf_op jit(solution)/shard_map/ppermute | solution.py:19
  52.4 1.9 collective-permute-start.1
  55.4 24.0 %collective-permute-done.1 = bf16[2,512,512]{2,1,0:T(8,128)(2,1)S(1)} collective-permute-done((bf16[2,512,512]{2,1,0:T(8,128)(2,1)S(1)}, bf16[2,512,512]{2,1,0:T(8,128)(2,1)S(1)}, u32[]{:S(2)}, u32[]{:S(2)}) %collective-permute-start.1) | collective-permute-done | bytes 1048608 | tf_op jit(solution)/shard_map/ppermute | solution.py:19
  79.4 1.6 maximum_maximum_fusion
  80.9 1.9 collective-permute-start.3
  84.7 1.7 copy.138
  86.4 1.6 pad_maximum_fusion.5
  88.0 1.8 copy.150
  94.6 34.3 %collective-permute-done.3 = bf16[2,1024,512]{2,1,0:T(8,128)(2,1)} collective-permute-done((bf16[2,1024,512]{2,1,0:T(8,128)(2,1)}, bf16[2,1024,512]{2,1,0:T(8,128)(2,1)}, u32[]{:S(2)}, u32[]{:S(2)}) %collective-permute-start.3) | collective-permute-done | bytes 2097184 | tf_op jit(solution)/shard_map/ppermute | solution.py:19
  129.0 1.7 constant_dynamic-update-slice_fusion.4
  131.0 1.9 copy-done.2
  133.8 1.7 reshape.547
  135.6 2.8 %fusion.4 = (f32[4,8,64]{2,1,0:T(8,128)S(1)}, f32[4,8,64,192]{3,2,1,0:T(8,128)S(1)}) fusion(pred[4,64,192]{2,1,0:T(8,128)(4,1)S(1)} %broadcast_and_fusion.1, bf16[192,4,8,64]{3,2,1,0:T(8,128)(2,1)} %reshape.547, bf16[64,4,8,64]{3,2,1,0:T(8,128)(2,1)} %bitcast.139), kind=kOutput, calls=%fused_computation.13 | convolution fusion | flops 51509248 | bytes 2678784 | tf_op jit(solution)/shard_map/qrhc,krhc->rhqk/dot_general | solution.py:51
  138.4 1.3 copy-done.10
  142.7 1.7 reshape.554
  144.3 4.3 %fusion.28 = f32[64,4,8,64]{0,3,2,1:T(8,128)} fusion(bf16[192,4,8,64]{3,2,1,0:T(8,128)(2,1)} %reshape.554, f32[4,8,64,192]{3,2,1,0:T(8,128)} %copy-done.10, f32[4,8,64]{2,1,0:T(8,128)S(1)} %get-tuple-element.31, pred[4,64,192]{2,1,0:T(8,128)(4,1)S(1)} %broadcast_and_fusion.1, f32[64,4,8]{0,2,1:T(8,128)S(1)} %bitcast.153), kind=kOutput, calls=%fused_computation.31 | convolution fusion | flops 52297728 | bytes 2949120 | tf_op jit(solution)/shard_map/rhqk,krhc->qrhc/dot_general | solution.py:66
  148.6 2.1 copy.156
  151.8 2.0 copy.157
  153.9 3.9 %slice_bitcast_fusion.1 = (bf16[2048,512]{1,0:T(8,128)(2,1)S(1)}, bf16[2048,512]{1,0:T(8,128)(2,1)}) fusion(bf16[2,2048,512]{2,1,0:T(8,128)(2,1)} %copy-done.2), kind=kLoop, calls=%fused_computation.7 | loop fusion | bytes 8388608 | tf_op jit(solution)/shard_map/squeeze | solution.py:102
  157.8 1.6 pad_maximum_fusion
  159.4 7.1 %reshape.549 = bf16[144,16,8,64]{3,2,1,0:T(8,128)(2,1)} reshape(bf16[2304,512]{1,0:T(8,128)(2,1)} %pad_maximum_fusion) | data formatting | bytes 4718592 | tf_op jit(solution)/shard_map/reshape | solution.py:43
  166.5 8.4 %fusion.5 = (f32[16,8,16]{2,1,0:T(8,128)S(1)}, f32[16,8,16,144]{3,2,1,0:T(8,128)}) fusion(pred[16,16,144]{2,1,0:T(8,128)(4,1)S(1)} %broadcast_and_fusion, bf16[144,16,8,64]{3,2,1,0:T(8,128)(2,1)} %reshape.549, bf16[16,16,8,64]{3,2,1,0:T(8,128)(2,1)S(1)} %bitcast.140), kind=kOutput, calls=%fused_computation.14 | convolution fusion | flops 38631424 | bytes 3846144 | tf_op jit(solution)/shard_map/qrhc,krhc->rhqk/dot_general | solution.py:51
  175.1 2.4 %fusion.9 = f32[16,8,16]{2,1,0:T(8,128)S(1)} fusion(f32[16,8,16,144]{3,2,1,0:T(8,128)} %get-tuple-element.30, f32[16,8,16]{2,1,0:T(8,128)S(1)} %get-tuple-element.29, pred[16,16,144]{2,1,0:T(8,128)(4,1)S(1)} %broadcast_and_fusion), kind=kLoop, calls=%fused_computation.18 | loop fusion | flops 1177600 | bytes 1232896 | tf_op jit(solution)/shard_map/reduce_sum | solution.py:65
  177.7 3.2 %pad_maximum_fusion.1 = bf16[2304,512]{1,0:T(8,128)(2,1)} fusion(bf16[256,512]{1,0:T(8,128)(2,1)S(1)} %copy-done.1, bf16[2048,512]{1,0:T(8,128)(2,1)} %get-tuple-element.10), kind=kLoop, calls=%fused_computation.5 | loop fusion | flops 4718592 | bytes 4718592 | tf_op jit(solution)/shard_map/concatenate | solution.py:103
  180.9 7.0 %reshape.556 = bf16[144,16,8,64]{3,2,1,0:T(8,128)(2,1)} reshape(bf16[2304,512]{1,0:T(8,128)(2,1)} %pad_maximum_fusion.1) | data formatting | bytes 4718592 | tf_op jit(solution)/shard_map/reshape | solution.py:44
  188.0 7.6 %fusion.53 = f32[16,16,8,64]{3,0,2,1:T(8,128)S(1)} fusion(bf16[144,16,8,64]{3,2,1,0:T(8,128)(2,1)} %reshape.556, f32[16,8,16,144]{3,2,1,0:T(8,128)} %get-tuple-element.30, f32[16,8,16]{2,1,0:T(8,128)S(1)} %get-tuple-element.29, pred[16,16,144]{2,1,0:T(8,128)(4,1)S(1)} %broadcast_and_fusion, f32[16,16,8]{0,2,1:T(8,128)S(1)} %bitcast.148), kind=kOutput, calls=%fused_computation.54 | convolution fusion | flops 39321600 | bytes 4116480 | tf_op jit(solution)/shard_map/rhqk,krhc->qrhc/dot_general | solution.py:66
  199.5 2.1 fusion.91
  201.6 10.3 %reduce-scatter.2.cloned.1.call-done = f32[128,2048]{1,0:T(8,128)} async-done(((f32[256,2048]{1,0:T(8,128)}), f32[128,2048]{1,0:T(8,128)}) %reduce-scatter.2.cloned.1.call-update) | async-done | bytes 1048592 | tf_op jit(solution)/shard_map/reduce_scatter | solution.py:119
  211.9 2.1 convert_element_type.114
  (93 shorter events, 24.0 us)
Async XLA Ops:
  6.5 193.0 %copy-start = (bf16[512,2048]{1,0:T(8,128)(2,1)S(1)}, bf16[512,2048]{1,0:T(8,128)(2,1)}, u32[]{:S(2)}) copy-start(bf16[512,2048]{1,0:T(8,128)(2,1)} %param.7) | copy-start | bytes 6291460
  6.5 205.4 %reduce-scatter.2.cloned.1.call-start = ((), (), s32[]{:S(2)}) async-start(), calls=%async_computation.1 | async-start | bytes 3145728 | tf_op jit(solution)/shard_map/reduce_scatter | solution.py:119
  7.8 2.4 %copy-start.1 = (bf16[256,512]{1,0:T(8,128)(2,1)S(1)}, bf16[256,512]{1,0:T(8,128)(2,1)}, u32[]{:S(2)}) copy-start(bf16[256,512]{1,0:T(8,128)(2,1)} %param.6) | copy-start | bytes 786436
  11.0 82.5 %collective-permute-start.2 = (bf16[2,256,512]{2,1,0:T(8,128)(2,1)}, bf16[2,256,512]{2,1,0:T(8,128)(2,1)}, u32[]{:S(2)}, u32[]{:S(2)}) collective-permute-start(bf16[2,256,512]{2,1,0:T(8,128)(2,1)} %pad_maximum_fusion.4), channel_id=1, source_target_pairs={{0,16},{2,18},{4,20},{6,22},{8,24},{10,26},{12,28},{14,30},{1,17},... | collective-permute-start | bytes 1572872 | tf_op jit(solution)/shard_map/ppermute | solution.py:19
  12.3 40.0 %collective-permute-start = (bf16[2,256,512]{2,1,0:T(8,128)(2,1)}, bf16[2,256,512]{2,1,0:T(8,128)(2,1)S(1)}, u32[]{:S(2)}, u32[]{:S(2)}) collective-permute-start(bf16[2,256,512]{2,1,0:T(8,128)(2,1)} %pad_maximum_fusion.4), channel_id=1, source_target_pairs={{0,2},{2,4},{4,6},{6,8},{8,10},{10,12},{12,14},{14,16},{16,18},{18... | collective-permute-start | bytes 1572872 | tf_op jit(solution)/shard_map/ppermute | solution.py:19
  19.2 35.1 %copy-start.5 = (bf16[256,8,64]{0,2,1:T(8,128)(2,1)S(1)}, bf16[256,8,64]{0,2,1:T(8,128)(2,1)}, u32[]{:S(2)}) copy-start(bf16[256,8,64]{0,2,1:T(8,128)(2,1)} %get-tuple-element.39) | copy-start | bytes 786436
  52.4 27.0 %collective-permute-start.1 = (bf16[2,512,512]{2,1,0:T(8,128)(2,1)S(1)}, bf16[2,512,512]{2,1,0:T(8,128)(2,1)S(1)}, u32[]{:S(2)}, u32[]{:S(2)}) collective-permute-start(bf16[2,512,512]{2,1,0:T(8,128)(2,1)S(1)} %maximum_maximum_fusion.1), channel_id=1, source_target_pairs={{0,4},{2,6},{4,8},{6,10},{8,12},{10,14},{12,16},{14,18},{16,20},{1... | collective-permute-start | bytes 3145736 | tf_op jit(solution)/shard_map/ppermute | solution.py:19
  55.1 27.8 %copy-start.15 = (f32[8,128]{1,0:T(8,128)}, f32[8,128]{1,0:T(8,128)S(1)}, u32[]{:S(2)}) copy-start(f32[8,128]{1,0:T(8,128)S(1)} %fusion.48) | copy-start | bytes 12292
  55.3 27.6 %copy-start.11 = (bf16[256,512]{0,1:T(8,128)(2,1)S(1)}, bf16[256,512]{0,1:T(8,128)(2,1)}, u32[]{:S(2)}) copy-start(bf16[256,512]{0,1:T(8,128)(2,1)} %copy.151) | copy-start | bytes 786436
  79.4 3.5 %copy-start.3 = (bf16[2,512,512]{2,1,0:T(8,128)(2,1)}, bf16[2,512,512]{2,1,0:T(8,128)(2,1)S(1)}, u32[]{:S(2)}) copy-start(bf16[2,512,512]{2,1,0:T(8,128)(2,1)S(1)} %collective-permute-done.1) | copy-start | bytes 3145732
  80.9 48.0 %collective-permute-start.3 = (bf16[2,1024,512]{2,1,0:T(8,128)(2,1)}, bf16[2,1024,512]{2,1,0:T(8,128)(2,1)}, u32[]{:S(2)}, u32[]{:S(2)}) collective-permute-start(bf16[2,1024,512]{2,1,0:T(8,128)(2,1)} %maximum_maximum_fusion), channel_id=1, source_target_pairs={{0,8},{2,10},{4,12},{6,14},{8,16},{10,18},{12,20},{14,22},{16,24},... | collective-permute-start | bytes 6291464 | tf_op jit(solution)/shard_map/ppermute | solution.py:19
  83.0 7.8 %copy-start.6 = (bf16[256,8,64]{0,2,1:T(8,128)(2,1)S(1)}, bf16[256,8,64]{0,2,1:T(8,128)(2,1)}, u32[]{:S(2)}) copy-start(bf16[256,8,64]{0,2,1:T(8,128)(2,1)} %get-tuple-element.39) | copy-start | bytes 786436
  89.8 2.6 %copy-start.12 = (bf16[256,512]{0,1:T(8,128)(2,1)S(1)}, bf16[256,512]{0,1:T(8,128)(2,1)}, u32[]{:S(2)}) copy-start(bf16[256,512]{0,1:T(8,128)(2,1)} %copy.150) | copy-start | bytes 786436
  90.8 2.0 copy-start.13
  92.4 38.3 %copy-start.17 = (f32[8,128]{1,0:T(8,128)}, f32[8,128]{1,0:T(8,128)S(1)}, u32[]{:S(2)}) copy-start(f32[8,128]{1,0:T(8,128)S(1)} %fusion.46) | copy-start | bytes 12292
  94.6 36.1 %copy-start.4 = (bf16[2,512,512]{2,1,0:T(8,128)(2,1)S(1)}, bf16[2,512,512]{2,1,0:T(8,128)(2,1)}, u32[]{:S(2)}) copy-start(bf16[2,512,512]{2,1,0:T(8,128)(2,1)} %copy-done.3) | copy-start | bytes 3145732
  130.9 2.9 %copy-start.7 = (bf16[256,512]{1,0:T(8,128)(2,1)S(1)}, bf16[256,512]{1,0:T(8,128)(2,1)}, u32[]{:S(2)}) copy-start(bf16[256,512]{1,0:T(8,128)(2,1)} %copy.140) | copy-start | bytes 786436
  131.0 2.0 copy-start.2
  138.4 1.3 copy-start.10
  153.9 3.9 %copy-start.8 = (bf16[256,512]{1,0:T(8,128)(2,1)S(1)}, bf16[256,512]{1,0:T(8,128)(2,1)}, u32[]{:S(2)}) copy-start(bf16[256,512]{1,0:T(8,128)(2,1)} %copy.140) | copy-start | bytes 786436
  159.4 7.1 %copy-start.9 = (bf16[256,8,64]{2,1,0:T(8,128)(2,1)S(1)}, bf16[256,8,64]{2,1,0:T(8,128)(2,1)}, u32[]{:S(2)}) copy-start(bf16[256,8,64]{2,1,0:T(8,128)(2,1)} %copy.139) | copy-start | bytes 786436
  195.5 2.7 %copy-start.14 = (f32[256,8]{0,1:T(8,128)S(1)}, f32[256,8]{0,1:T(8,128)}, u32[]{:S(2)}) copy-start(f32[256,8]{0,1:T(8,128)} %copy.144) | copy-start | bytes 24580
  195.5 2.7 %copy-start.16 = (f32[8,128]{1,0:T(8,128)S(1)}, f32[8,128]{1,0:T(8,128)}, u32[]{:S(2)}) copy-start(f32[8,128]{1,0:T(8,128)} %copy-done.15) | copy-start | bytes 12292
  195.5 2.7 %copy-start.18 = (f32[8,128]{1,0:T(8,128)S(1)}, f32[8,128]{1,0:T(8,128)}, u32[]{:S(2)}) copy-start(f32[8,128]{1,0:T(8,128)} %copy-done.17) | copy-start | bytes 12292
Sparse Core Ops, SparseCore 0:
  201.7 10.1 reduce-scatter.1
where the time goes:
time: 223 us; the launch traced here: 221 us
  waiting for transfers between devices  101 us (45%)
  local copies, waits for them, and re-layouts  48.3 us (22%)
  matrix products  28.2 us (13%)
  other arithmetic  21.3 us (10%)
  between operations  13.9 us (6%)
  starting transfers between devices  8.23 us (4%)
    ppermute x4, waiting for transfers between devices, shifted(): lax.ppermute(value, axis, [(source, source + steps) for source in range(i...  90.7 us
    dot_general x4, matrix products, pattern_part(): jnp.einsum('rhqk,krhc->qrhc', weights.astype(jnp.bfloat16), value_part, p...  13.3 us
    dot_general x4, matrix products, pattern_part(): jnp.einsum('qrhc,krhc->rhqk', query_sub[first_row:first_row + block_rows]...  12.9 us
    reduce_scatter x1, waiting for transfers between devices, per_device(): lax.psum_scatter(jnp.dot(mixed, out_weight, preferred_element_type=jnp.fl...  10.3 us
    reshape x2, local copies, waits for them, and re-layouts, pattern_part(): key_sub = key_ext.reshape(BACK + length, dilation, head_count, HD)  8.84 us
    reshape x2, local copies, waits for them, and re-layouts, pattern_part(): value_sub = value_ext.reshape(BACK + length, dilation, head_count, HD)  8.74 us
    ppermute x4, starting transfers between devices, shifted(): lax.ppermute(value, axis, [(source, source + steps) for source in range(i...  8.23 us
    squeeze x4, local copies, waits for them, and re-layouts, per_device(): prior[0, prior.shape[1] - reach:]  7.16 us
  transfers between devices with their start and end apart: 5, of which 4 were waited for; matrix products, arithmetic and copies ran while one was open for 8% of the time, Pallas kernels for 0%

commit v1 on v0

v1 whole, which is shorter than its diff:
```python
import functools
import math

import jax
import jax.numpy as jnp
import numpy as np
from jax import lax
from jax.experimental import pallas as pl
from jax.experimental.pallas import tpu as pltpu
from jax.sharding import PartitionSpec as P

HD = 64
BACK = 128
THETA = 500000.0
FAR = -1e30
F32 = jnp.float32
BF16 = jnp.bfloat16
LANES = 2 * HD
NT = (((1,), (1,)), ((), ()))


def place(p):
    return ((p & 7) << 4) + (((p >> 3) & 3) << 2) + (p >> 5)


def iota(shape, axis):
    return lax.broadcasted_iota(jnp.int32, shape, axis)


def kernel(
    G, ngroups, tp_count,
    q_ref, k_ref, v_ref, cosb_ref, sinb_ref, inv_ref, w_ref, out_ref,
    qs, kvs, qr, kv, kvf, q2, q2f, acc, top, bias, wbuf, rs, rr, mx,
    s_kv, s_q, s_x, r_kv, r_q, r_x, w_sem, s_ret, r_ret,
):
    sp = lax.axis_index("sp")
    tp = lax.axis_index("tp")
    group = sp // G
    me = sp - group * G
    base = group * G
    has_prev = group > 0
    has_next = group < ngroups - 1
    seat = me * tp_count + tp
    seats = G * tp_count
    head = tp * G + me
    tok = q_ref.shape[0]
    halves = tok // BACK

    def target(s, t):
        return {"sp": s, "tp": t}

    barrier = pltpu.get_barrier_semaphore()
    for o in range(1, seats):
        n = lax.rem(seat + o, seats)
        pl.semaphore_signal(
            barrier, inc=1, device_id=target(base + n // tp_count, lax.rem(n, tp_count)),
            device_id_type=pl.DeviceIdType.MESH,
        )

    @pl.when(has_prev)
    def _():
        for o in range(G):
            pl.semaphore_signal(
                barrier, inc=1, device_id=target(base - G + o, tp),
                device_id_type=pl.DeviceIdType.MESH,
            )

    @pl.when(has_next)
    def _():
        for o in range(G):
            pl.semaphore_signal(
                barrier, inc=1, device_id=target(base + G + o, tp),
                device_id_type=pl.DeviceIdType.MESH,
            )

    w_local = pltpu.make_async_copy(w_ref, wbuf.at[tp], w_sem.at[0])
    w_local.start()

    lane = iota((BACK, LANES), 1)
    low = lane < HD
    lane_t = iota((tok, LANES), 1)
    first = (lane_t & (HD - 1)) < HD // 2
    angle = inv_ref[...] * (sp * tok).astype(F32)
    ca = jnp.cos(angle)[:1]
    sa = jnp.sin(angle)[:1]
    cos = ca * cosb_ref[...] - sa * sinb_ref[...]
    sin = sa * cosb_ref[...] + ca * sinb_ref[...]
    sin = jnp.where(first, -sin, sin)
    swizzle = jnp.where(place(iota((BACK, BACK), 0)) == iota((BACK, BACK), 1), 1.0, 0.0).astype(BF16)
    back = jnp.where(place(iota((BACK, BACK), 1)) == iota((BACK, BACK), 0), 1.0, 0.0).astype(BF16)

    def turn(ref, cols):
        x = ref[:, cols].astype(F32)
        other = jnp.where(first, pltpu.roll(x, LANES - HD // 2, 1), pltpu.roll(x, HD // 2, 1))
        return (x * cos + other * sin).astype(BF16)

    def sw(x):
        return jnp.dot(swizzle, x, preferred_element_type=F32)

    for m in range(G // 2):
        cols = slice(m * LANES, (m + 1) * LANES)
        tq = turn(q_ref, cols)
        tk = turn(k_ref, cols)
        tv = v_ref[:, cols]
        qa = sw(tq[:BACK]) * (1.0 / math.sqrt(HD))
        qb = sw(tq[BACK:]) * (1.0 / math.sqrt(HD))
        qs[2 * m] = jnp.where(low, qa, pltpu.roll(qb, HD, 1)).astype(BF16)
        qs[2 * m + 1] = jnp.where(low, pltpu.roll(qa, HD, 1), qb).astype(BF16)
        for e in range(halves):
            ks = sw(tk[e * BACK : (e + 1) * BACK])
            vs = sw(tv[e * BACK : (e + 1) * BACK])
            kvs[2 * m, e] = jnp.where(low, ks, pltpu.roll(vs, HD, 1)).astype(BF16)
            kvs[2 * m + 1, e] = jnp.where(low, pltpu.roll(ks, HD, 1), vs).astype(BF16)

    pl.semaphore_wait(
        barrier, seats - 1 + jnp.where(has_prev, G, 0) + jnp.where(has_next, G, 0)
    )

    own0 = G * halves

    def copy_kv(dest):
        return pltpu.make_async_remote_copy(
            src_ref=kvs.at[dest], dst_ref=kv.at[pl.ds(own0 + halves * me, halves)],
            send_sem=s_kv.at[dest], recv_sem=r_kv.at[me],
            device_id=target(base + dest, tp), device_id_type=pl.DeviceIdType.MESH,
        )

    def copy_q(dest):
        return pltpu.make_async_remote_copy(
            src_ref=qs.at[dest], dst_ref=qr.at[me],
            send_sem=s_q.at[dest], recv_sem=r_q.at[me],
            device_id=target(base + dest, tp), device_id_type=pl.DeviceIdType.MESH,
        )

    def copy_x(dest):
        return pltpu.make_async_remote_copy(
            src_ref=kvs.at[dest], dst_ref=kv.at[pl.ds(halves * me, halves)],
            send_sem=s_x.at[dest], recv_sem=r_x.at[me],
            device_id=target(base + G + dest, tp), device_id_type=pl.DeviceIdType.MESH,
        )

    w_away = pltpu.make_async_remote_copy(
        src_ref=w_ref, dst_ref=wbuf.at[tp], send_sem=w_sem.at[1], recv_sem=w_sem.at[2],
        device_id=target(sp, tp_count - 1 - tp), device_id_type=pl.DeviceIdType.MESH,
    )

    for o in range(1, G):
        copy_kv(lax.rem(me + o, G)).start()
        copy_q(lax.rem(me + o, G)).start()

    @pl.when(has_next)
    def _():
        for o in range(G):
            copy_x(lax.rem(me + o, G)).start()

    w_away.start()

    row = iota((BACK, 2 * BACK), 0)
    col = iota((BACK, 2 * BACK), 1)
    old = col < BACK
    missing = jnp.logical_and(old, group == 0)

    def stride4(n):
        w = n & 31
        return ((n >> 5) << 5) + ((w & 7) << 2) + (w >> 3)

    def masked(distance):
        return jnp.where((distance >= 0) & (distance <= BACK), 0.0, FAR)

    b1 = masked(place(row) + BACK - place(col & (BACK - 1)) - ((col >> 7) << 7))
    b4 = masked(stride4(row) + BACK - stride4(col))
    b16 = masked(row + BACK - col)
    bias[0] = b1
    bias[1] = b4
    bias[2] = jnp.where(missing, FAR, b1)
    bias[3] = jnp.where(missing, FAR, b4)
    bias[4] = jnp.where(missing, FAR, b16)

    acc[...] = jnp.zeros_like(acc)
    top[...] = jnp.full_like(top, FAR)

    @pl.when(jnp.logical_not(has_prev))
    def _():
        kv[:own0] = jnp.zeros((own0, BACK, LANES), BF16)

    kv[pl.ds(own0 + halves * me, halves)] = kvs[me]
    qr[me] = qs[me]

    def ready(s):
        x = qr[s].astype(F32)
        a = jnp.where(low, x, 0.0)
        b = jnp.where(low, pltpu.roll(x, HD, 1), 0.0)
        q2f[2 * s] = a
        q2f[2 * s + 1] = b
        q2[2 * s] = a.astype(BF16)
        q2[2 * s + 1] = b.astype(BF16)
        at = pl.ds(own0 + halves * s, halves)
        kvf[at] = kv[at].astype(F32)

    ready(me)
    for o in range(1, G):
        s = lax.rem(me - o + G, G)
        pltpu.make_async_remote_copy(
            src_ref=kvs.at[s], dst_ref=kv.at[pl.ds(own0 + halves * s, halves)],
            send_sem=s_kv.at[s], recv_sem=r_kv.at[s],
            device_id=target(base + s, tp), device_id_type=pl.DeviceIdType.MESH,
        ).wait_recv()
        pltpu.make_async_remote_copy(
            src_ref=qs.at[s], dst_ref=qr.at[s],
            send_sem=s_q.at[s], recv_sem=r_q.at[s],
            device_id=target(base + s, tp), device_id_type=pl.DeviceIdType.MESH,
        ).wait_recv()
        ready(s)

    low_keys = iota((2 * BACK, LANES), 1) < HD

    def attend(q, keys, b, o_old, t_old):
        s = lax.dot_general(q, keys, NT, preferred_element_type=F32) + b
        t_new = jnp.maximum(t_old, jnp.max(s, axis=1, keepdims=True))
        p = jnp.concatenate(
            [jnp.exp(s[:, :BACK] - t_new), jnp.exp(s[:, BACK:] - t_new)], axis=1
        ).astype(BF16)
        ones = jnp.where(low_keys, jnp.ones_like(keys), keys)
        o = jnp.dot(p, ones, preferred_element_type=F32)
        return o_old * jnp.exp(t_old - t_new) + o, t_new

    def run(tiles):
        done = []
        for q, keys, b, where in tiles:
            shape = acc[where].shape
            o, t = attend(
                q, keys, b, acc[where].reshape(BACK, LANES), top[where].reshape(BACK, LANES)
            )
            done.append((where, o.reshape(shape), t.reshape(shape)))
        for where, o, t in done:
            acc[where] = o
            top[where] = t

    def tile1(h, b):
        return (
            q2[h], kv[pl.ds(own0 - 1 + h, 2)].reshape(2 * BACK, LANES), bias[b], (h,),
        )

    def tile4(quarter, r, b):
        rows = pl.ds(r * 32, 32)
        return (
            q2[4 * quarter : 4 * quarter + 4, rows, :].reshape(BACK, LANES),
            kv[own0 + 4 * quarter - 4 : own0 + 4 * quarter + 4, rows, :].reshape(2 * BACK, LANES),
            bias[b],
            (slice(4 * quarter, 4 * quarter + 4), rows, slice(None)),
        )

    def tile16(r):
        rows = pl.ds(r * 8, 8)
        return (
            q2f[:, rows, :].reshape(BACK, LANES).astype(BF16),
            kvf[:, rows, :].reshape(2 * BACK, LANES).astype(BF16),
            bias[4],
            (slice(None), rows, slice(None)),
        )

    nq = G * halves

    @pl.loop(0, (nq - 1) // 3)
    def _(i):
        run([tile1(1 + 3 * i + n, 0) for n in range(3)])

    @pl.loop(0, 4)
    def _(r):
        run([tile4(n, r, 1) for n in range(1, nq // 4)])

    @pl.when(has_prev)
    def _():
        for o in range(G):
            s = lax.rem(me - o + G, G)
            pltpu.make_async_remote_copy(
                src_ref=kvs.at[s], dst_ref=kv.at[pl.ds(halves * s, halves)],
                send_sem=s_x.at[s], recv_sem=r_x.at[s],
                device_id=target(base - G + s, tp), device_id_type=pl.DeviceIdType.MESH,
            ).wait_recv()

    @pl.loop(0, G)
    def _(i):
        at = pl.ds(2 * i, 2)
        kvf[at] = kv[at].astype(F32)

    run([tile1(0, 2)])
    run([tile4(0, r, 3) for r in range(4)])

    @pl.loop(0, 4)
    def _(i):
        run([tile16(4 * i + n) for n in range(4)])

    @pl.loop(0, nq)
    def _(h):
        o = acc[h]
        y = o / pltpu.roll(o, HD, 1)
        rs[h] = jnp.where(low[: HD], pltpu.roll(y[:HD], HD, 1), y[HD:]).astype(BF16)

    def copy_ret(n):
        return pltpu.make_async_remote_copy(
            src_ref=rs.at[n], dst_ref=rr.at[head], send_sem=s_ret.at[n], recv_sem=r_ret.at[head],
            device_id=target(base + n // tp_count, lax.rem(n, tp_count)),
            device_id_type=pl.DeviceIdType.MESH,
        )

    for o in range(1, seats):
        copy_ret(lax.rem(seat + o, seats)).start()
    rr[head] = rs[seat]

    for o in range(1, G):
        copy_kv(lax.rem(me + o, G)).wait_send()
        copy_q(lax.rem(me + o, G)).wait_send()

    @pl.when(has_next)
    def _():
        for o in range(G):
            copy_x(lax.rem(me + o, G)).wait_send()

    w_local.wait()
    w_away.wait_send()
    pltpu.make_async_remote_copy(
        src_ref=w_ref, dst_ref=wbuf.at[tp_count - 1 - tp],
        send_sem=w_sem.at[1], recv_sem=w_sem.at[2],
        device_id=target(sp, tp_count - 1 - tp), device_id_type=pl.DeviceIdType.MESH,
    ).wait_recv()

    for o in range(1, seats):
        n = lax.rem(seat - o + seats, seats)
        their = lax.rem(n, tp_count) * G + n // tp_count
        pltpu.make_async_remote_copy(
            src_ref=rs.at[n], dst_ref=rr.at[their], send_sem=s_ret.at[n],
            recv_sem=r_ret.at[their],
            device_id=target(base + n // tp_count, lax.rem(n, tp_count)),
            device_id_type=pl.DeviceIdType.MESH,
        ).wait_recv()

    low_h = low[:HD]
    for m in range(seats // 2):
        x0 = rr[2 * m].astype(F32)
        x1 = rr[2 * m + 1].astype(F32)
        pair = jnp.concatenate(
            [jnp.where(low_h, x0, pltpu.roll(x1, HD, 1)), jnp.where(low_h, pltpu.roll(x0, HD, 1), x1)],
            axis=0,
        ).astype(BF16)
        mx[:, m * LANES : (m + 1) * LANES] = jnp.dot(
            back, pair, preferred_element_type=F32
        ).astype(BF16)

    width = wbuf.shape[1]
    step = 512

    @pl.loop(0, out_ref.shape[1] // step)
    def _(c):
        cols = pl.ds(pl.multiple_of(c * step, step), step)
        total = jnp.dot(mx[:, :width], wbuf[0, :, cols], preferred_element_type=F32)
        total = total + jnp.dot(mx[:, width:], wbuf[1, :, cols], preferred_element_type=F32)
        out_ref[:, cols] = total.astype(BF16)

    for o in range(1, seats):
        copy_ret(lax.rem(seat + o, seats)).wait_send()


def per_device(sp_count, tp_count, query_rows, key_rows, value_rows, out_weight):
    tok = query_rows.shape[0]
    G = query_rows.shape[1] // HD
    halves = tok // BACK
    ngroups = sp_count // G
    assert tok == 2 * BACK and tp_count == 2 and sp_count % G == 0
    assert G * tok == 16 * BACK
    inverse = np.power(THETA, -np.arange(HD // 2) / (HD // 2))
    inverse = np.tile(inverse, LANES // (HD // 2))[None, :]
    local = np.arange(tok)[:, None] * inverse
    cosb = jnp.asarray(np.cos(local), F32)
    sinb = jnp.asarray(np.sin(local), F32)
    inv = jnp.asarray(np.tile(inverse, (8, 1)), F32)
    seats = G * tp_count
    vmem = pl.BlockSpec(memory_space=pltpu.VMEM)
    dma = pltpu.SemaphoreType.DMA
    return pl.pallas_call(
        functools.partial(kernel, G, ngroups, tp_count),
        out_shape=jax.ShapeDtypeStruct((tok // tp_count, out_weight.shape[1]), BF16),
        in_specs=[vmem] * 6 + [pl.BlockSpec(memory_space=pl.ANY)],
        out_specs=vmem,
        scratch_shapes=[
            pltpu.VMEM((G, BACK, LANES), BF16),
            pltpu.VMEM((G, halves, BACK, LANES), BF16),
            pltpu.VMEM((G, BACK, LANES), BF16),
            pltpu.VMEM((2 * G * halves, BACK, LANES), BF16),
            pltpu.VMEM((2 * G * halves, BACK, LANES), F32),
            pltpu.VMEM((G * halves, BACK, LANES), BF16),
            pltpu.VMEM((G * halves, BACK, LANES), F32),
            pltpu.VMEM((G * halves, BACK, LANES), F32),
            pltpu.VMEM((G * halves, BACK, LANES), F32),
            pltpu.VMEM((5, BACK, 2 * BACK), F32),
            pltpu.VMEM((tp_count,) + out_weight.shape, BF16),
            pltpu.VMEM((seats, HD, LANES), BF16),
            pltpu.VMEM((seats, HD, LANES), BF16),
            pltpu.VMEM((BACK, seats * HD), BF16),
            dma((G,)), dma((G,)), dma((G,)), dma((G,)), dma((G,)), dma((G,)),
            dma((3,)), dma((seats,)), dma((seats,)),
        ],
        compiler_params=pltpu.CompilerParams(
            collective_id=0, has_side_effects=True, vmem_limit_bytes=48 * 1024 * 1024
        ),
    )(query_rows, key_rows, value_rows, cosb, sinb, inv, out_weight)


def solution(mesh):
    return jax.shard_map(
        functools.partial(per_device, mesh.shape["sp"], mesh.shape["tp"]),
        mesh=mesh,
        in_specs=(P("sp", "tp"), P("sp", "tp"), P("sp", "tp"), P("tp", None)),
        out_specs=P(("sp", "tp"), None),
        check_vma=False,
    )
```

time: 223 us -> 50.6 us (0.23)
  waiting for transfers between devices: 101 us -> 0 us
  Pallas kernels: 0 us -> 41.9 us
  local copies, waits for them, and re-layouts: 48.3 us -> 7.73 us
  matrix products: 28.2 us -> 0 us
  other arithmetic: 21.3 us -> 0 us
  between operations: 13.9 us -> 0.02 us
  starting transfers between devices: 8.23 us -> 0 us
    ppermute x4 -> x0, waiting for transfers between devices: 90.7 us -> none  [shifted(): lax.ppermute(value, axis, [(source, source + steps) for source in range(i...]
    pallas_call x0 -> x1, Pallas kernels: none -> 41.9 us  [per_device(): pl.pallas_call(functools.partial(kernel, G, ngroups, tp_count), out_shape...]
    dot_general x9 -> x0, matrix products: 28.2 us -> none  [the longest x4 13.3 us: pattern_part(): jnp.einsum('rhqk,krhc->qrhc', weights.astype(jnp.bfloat16), value_part, p...]
    reshape x10 -> x0, local copies, waits for them, and re-layouts: 20.8 us -> none  [the longest x2 8.84 us: pattern_part(): key_sub = key_ext.reshape(BACK + length, dilation, head_count, HD)]
    convert_element_type x9 -> x0, local copies, waits for them, and re-layouts: 10.9 us -> none  [the longest x3 5.25 us: per_device(): weighted = weighted + scales[1][..., None] * results[1].astype(jnp.float32)]
    concatenate x9 -> x0, other arithmetic: 10.9 us -> none  [the longest x3 5.9 us: per_device(): jnp.concatenate([prior[1, prior.shape[1] - reach:], value_rows], axis=0)]
    reduce_scatter x1 -> x0, waiting for transfers between devices: 10.3 us -> none  [per_device(): lax.psum_scatter(jnp.dot(mixed, out_weight, preferred_element_type=jnp.fl...]
    ppermute x4 -> x0, starting transfers between devices: 8.23 us -> none  [shifted(): lax.ppermute(value, axis, [(source, source + steps) for source in range(i...]
  transfers between devices with their start and end apart: 5 -> 0, of which waited for: 4 -> 0; matrix products, arithmetic and copies ran while one was open for 8% -> 0% of each run, Pallas kernels for 0% -> 0%
where the time goes in v1:
time: 50.6 us; the launch traced here: 49.7 us
  Pallas kernels  41.9 us (83%)
  local copies, waits for them, and re-layouts  7.73 us (15%)
    pallas_call x1, Pallas kernels, per_device(): pl.pallas_call(functools.partial(kernel, G, ngroups, tp_count), out_shape...  41.9 us
    unnamed x15, local copies, waits for them, and re-layouts  7.73 us

profile of v1, /device:TPU:17, one launch (start us, length us, event | category | flops | bytes accessed | tf_op | source)
XLA Modules:
  0.0 49.7 jit_solution(5990681217935102239)
XLA Ops:
  0.0 0.0 copy-start
  0.0 1.6 %copy-done = bf16[512,2048]{1,0:T(8,128)(2,1)S(1)} copy-done((bf16[512,2048]{1,0:T(8,128)(2,1)S(1)}, bf16[512,2048]{1,0:T(8,128)(2,1)}, u32[]{:S(2)}) %copy-start) | copy-done | bytes 2097176
  1.6 0.0 copy-start.1
  1.6 0.9 %copy-done.1 = bf16[256,512]{1,0:T(8,128)(2,1)S(1)} copy-done((bf16[256,512]{1,0:T(8,128)(2,1)S(1)}, bf16[256,512]{1,0:T(8,128)(2,1)}, u32[]{:S(2)}) %copy-start.1) | copy-done | bytes 262168
  2.5 0.0 copy-start.2
  2.5 0.9 %copy-done.2 = bf16[256,512]{1,0:T(8,128)(2,1)S(1)} copy-done((bf16[256,512]{1,0:T(8,128)(2,1)S(1)}, bf16[256,512]{1,0:T(8,128)(2,1)}, u32[]{:S(2)}) %copy-start.2) | copy-done | bytes 262168
  3.5 0.0 copy-start.3
  3.5 0.9 %copy-done.3 = bf16[256,512]{1,0:T(8,128)(2,1)S(1)} copy-done((bf16[256,512]{1,0:T(8,128)(2,1)S(1)}, bf16[256,512]{1,0:T(8,128)(2,1)}, u32[]{:S(2)}) %copy-start.3) | copy-done | bytes 262168
  4.4 0.0 copy-start.4
  4.4 0.9 %copy-done.4 = f32[256,128]{1,0:T(8,128)S(1)} copy-done((f32[256,128]{1,0:T(8,128)S(1)}, f32[256,128]{1,0:T(8,128)}, u32[]{:S(2)}) %copy-start.4) | copy-done | bytes 131096
  5.3 0.0 copy-start.5
  5.4 0.9 %copy-done.5 = f32[256,128]{1,0:T(8,128)S(1)} copy-done((f32[256,128]{1,0:T(8,128)S(1)}, f32[256,128]{1,0:T(8,128)}, u32[]{:S(2)}) %copy-start.5) | copy-done | bytes 131096
  6.3 0.0 copy-start.6
  6.3 0.7 %copy-done.6 = f32[8,128]{1,0:T(8,128)S(1)} copy-done((f32[8,128]{1,0:T(8,128)S(1)}, f32[8,128]{1,0:T(8,128)}, u32[]{:S(2)}) %copy-start.6) | copy-done | bytes 4120
  6.9 41.9 %shard_map.73 = bf16[128,2048]{1,0:T(8,128)(2,1)S(1)} custom-call(bf16[256,512]{1,0:T(8,128)(2,1)S(1)} %copy-done.1, bf16[256,512]{1,0:T(8,128)(2,1)S(1)} %copy-done.2, bf16[256,512]{1,0:T(8,128)(2,1)S(1)} %copy-done.3, f32[256,128]{1,0:T(8,128)S(1)} %copy-done.5, f32[256,128]{1,0:T(8,128)S(1)} %copy-done.4, f32[8,128]{1,0:T(8,128)S(1)} %copy-done.6, ...), custom_call_target="tpu_custom_call" | custom-call | tf_op jit(solution)/shard_map/pallas_call | solution.py:380
  48.9 0.8 %copy.9 = bf16[128,2048]{1,0:T(8,128)(2,1)} copy(bf16[128,2048]{1,0:T(8,128)(2,1)S(1)} %shard_map.73) | data formatting | bytes 1048576
Async XLA Ops:
  0.0 1.6 %copy-start = (bf16[512,2048]{1,0:T(8,128)(2,1)S(1)}, bf16[512,2048]{1,0:T(8,128)(2,1)}, u32[]{:S(2)}) copy-start(bf16[512,2048]{1,0:T(8,128)(2,1)} %w_ref.1) | copy-start | bytes 6291460
  1.6 0.9 %copy-start.1 = (bf16[256,512]{1,0:T(8,128)(2,1)S(1)}, bf16[256,512]{1,0:T(8,128)(2,1)}, u32[]{:S(2)}) copy-start(bf16[256,512]{1,0:T(8,128)(2,1)} %q_ref.1) | copy-start | bytes 786436
  2.5 0.9 %copy-start.2 = (bf16[256,512]{1,0:T(8,128)(2,1)S(1)}, bf16[256,512]{1,0:T(8,128)(2,1)}, u32[]{:S(2)}) copy-start(bf16[256,512]{1,0:T(8,128)(2,1)} %k_ref.1) | copy-start | bytes 786436
  3.5 0.9 %copy-start.3 = (bf16[256,512]{1,0:T(8,128)(2,1)S(1)}, bf16[256,512]{1,0:T(8,128)(2,1)}, u32[]{:S(2)}) copy-start(bf16[256,512]{1,0:T(8,128)(2,1)} %v_ref.1) | copy-start | bytes 786436
  4.4 0.9 %copy-start.4 = (f32[256,128]{1,0:T(8,128)S(1)}, f32[256,128]{1,0:T(8,128)}, u32[]{:S(2)}) copy-start(f32[256,128]{1,0:T(8,128)} %constant.7.clone.sinb_ref) | copy-start | bytes 393220
  5.3 0.9 %copy-start.5 = (f32[256,128]{1,0:T(8,128)S(1)}, f32[256,128]{1,0:T(8,128)}, u32[]{:S(2)}) copy-start(f32[256,128]{1,0:T(8,128)} %constant.6.clone.cosb_ref) | copy-start | bytes 393220
  6.3 0.7 %copy-start.6 = (f32[8,128]{1,0:T(8,128)S(1)}, f32[8,128]{1,0:T(8,128)}, u32[]{:S(2)}) copy-start(f32[8,128]{1,0:T(8,128)} %constant.8.clone.inv_ref) | copy-start | bytes 12292

commit v2 on v1

--- a/solution.py
+++ b/solution.py
@@ -29,10 +29,19 @@
 
 def kernel(
     G, ngroups, tp_count,
-    q_ref, k_ref, v_ref, cosb_ref, sinb_ref, inv_ref, w_ref, out_ref,
-    qs, kvs, qr, kv, kvf, q2, q2f, acc, top, bias, wbuf, rs, rr, mx,
-    s_kv, s_q, s_x, r_kv, r_q, r_x, w_sem, s_ret, r_ret,
+    q_hbm, k_hbm, v_hbm, cosb_hbm, sinb_hbm, inv_hbm, w_ref, out_ref,
+    q_ref, k_ref, v_ref, cosb_ref, sinb_ref, inv_ref, qs, kvs, qr, kv, kvf, q2, q2f, acc, top, bias, wbuf, rs, rr, mx,
+    s_kv, s_q, s_x, r_kv, r_q, r_x, w_sem, s_ret, r_ret, in_sem,
 ):
+    loads = [
+        pltpu.make_async_copy(source, dest, in_sem.at[n])
+        for n, (source, dest) in enumerate((
+            (inv_hbm, inv_ref), (cosb_hbm, cosb_ref), (sinb_hbm, sinb_ref),
+            (k_hbm, k_ref), (v_hbm, v_ref), (q_hbm, q_ref),
+        ))
+    ]
+    for load in loads:
+        load.start()
     sp = lax.axis_index("sp")
     tp = lax.axis_index("tp")
     group = sp // G
@@ -75,6 +84,9 @@
 
     w_local = pltpu.make_async_copy(w_ref, wbuf.at[tp], w_sem.at[0])
     w_local.start()
+
+    for load in loads:
+        load.wait()
 
     lane = iota((BACK, LANES), 1)
     low = lane < HD
@@ -380,9 +392,15 @@
     return pl.pallas_call(
         functools.partial(kernel, G, ngroups, tp_count),
         out_shape=jax.ShapeDtypeStruct((tok // tp_count, out_weight.shape[1]), BF16),
-        in_specs=[vmem] * 6 + [pl.BlockSpec(memory_space=pl.ANY)],
+        in_specs=[pl.BlockSpec(memory_space=pl.ANY)] * 7,
         out_specs=vmem,
         scratch_shapes=[
+            pltpu.VMEM(query_rows.shape, BF16),
+            pltpu.VMEM(query_rows.shape, BF16),
+            pltpu.VMEM(query_rows.shape, BF16),
+            pltpu.VMEM(cosb.shape, F32),
+            pltpu.VMEM(sinb.shape, F32),
+            pltpu.VMEM(inv.shape, F32),
             pltpu.VMEM((G, BACK, LANES), BF16),
             pltpu.VMEM((G, halves, BACK, LANES), BF16),
             pltpu.VMEM((G, BACK, LANES), BF16),
@@ -398,10 +416,10 @@
             pltpu.VMEM((seats, HD, LANES), BF16),
             pltpu.VMEM((BACK, seats * HD), BF16),
             dma((G,)), dma((G,)), dma((G,)), dma((G,)), dma((G,)), dma((G,)),
-            dma((3,)), dma((seats,)), dma((seats,)),
+            dma((3,)), dma((seats,)), dma((seats,)), dma((6,)),
         ],
         compiler_params=pltpu.CompilerParams(
-            collective_id=0, has_side_effects=True, vmem_limit_bytes=48 * 1024 * 1024
+            collective_id=0, has_side_effects=True, vmem_limit_bytes=63 * 1024 * 1024
         ),
     )(query_rows, key_rows, value_rows, cosb, sinb, inv, out_weight)
 

time: 50.6 us -> 45.3 us (0.90)
  local copies, waits for them, and re-layouts: 7.73 us -> 1.88 us
  Pallas kernels: 41.9 us -> 42.7 us
    unnamed x15 -> x1, local copies, waits for them, and re-layouts: 7.73 us -> 1.88 us
    pallas_call x1, Pallas kernels: 41.9 us -> 42.7 us  [per_device(): pl.pallas_call(functools.partial(kernel, G, ngroups, tp_count), out_shape...]
where the time goes in v2:
time: 45.3 us; the launch traced here: 44.6 us
  Pallas kernels  42.7 us (94%)
  local copies, waits for them, and re-layouts  1.88 us (4%)
    pallas_call x1, Pallas kernels, per_device(): pl.pallas_call(functools.partial(kernel, G, ngroups, tp_count), out_shape...  42.7 us
    unnamed x1, local copies, waits for them, and re-layouts  1.88 us

profile of v2, /device:TPU:17, one launch (start us, length us, event | category | flops | bytes accessed | tf_op | source)
XLA Modules:
  0.0 44.6 jit_solution(17679751564471427289)
XLA Ops:
  0.0 42.7 %shard_map.73 = bf16[128,2048]{1,0:T(8,128)(2,1)} custom-call(bf16[256,512]{1,0:T(8,128)(2,1)} %q_hbm.1, bf16[256,512]{1,0:T(8,128)(2,1)} %k_hbm.1, bf16[256,512]{1,0:T(8,128)(2,1)} %v_hbm.1, f32[256,128]{1,0:T(8,128)} %constant.6.clone.cosb_hbm, f32[256,128]{1,0:T(8,128)} %constant.7.clone.sinb_hbm, f32[8,128]{1,0:T(8,128)} %constant.8.clone.inv_hbm, ...), custom_call_target="tpu_custom_call" | custom-call | tf_op jit(solution)/shard_map/pallas_call | solution.py:392
  42.7 1.9 %copy.9 = bf16[128,2048]{1,0:T(8,128)(2,1)} copy(bf16[128,2048]{1,0:T(8,128)(2,1)} %shard_map.73) | data formatting | bytes 1048576

commit v3 on v2

--- a/solution.py
+++ b/solution.py
@@ -109,8 +109,51 @@
     def sw(x):
         return jnp.dot(swizzle, x, preferred_element_type=F32)
 
-    for m in range(G // 2):
-        cols = slice(m * LANES, (m + 1) * LANES)
+    own0 = G * halves
+
+    def copy_kv(dest):
+        return pltpu.make_async_remote_copy(
+            src_ref=kvs.at[dest], dst_ref=kv.at[pl.ds(own0 + halves * me, halves)],
+            send_sem=s_kv.at[dest], recv_sem=r_kv.at[me],
+            device_id=target(base + dest, tp), device_id_type=pl.DeviceIdType.MESH,
+        )
+
+    def copy_q(dest):
+        return pltpu.make_async_remote_copy(
+            src_ref=qs.at[dest], dst_ref=qr.at[me],
+            send_sem=s_q.at[dest], recv_sem=r_q.at[me],
+            device_id=target(base + dest, tp), device_id_type=pl.DeviceIdType.MESH,
+        )
+
+    def copy_x(dest):
+        return pltpu.make_async_remote_copy(
+            src_ref=kvs.at[dest], dst_ref=kv.at[pl.ds(halves * me, halves)],
+            send_sem=s_x.at[dest], recv_sem=r_x.at[me],
+            device_id=target(base + G + dest, tp), device_id_type=pl.DeviceIdType.MESH,
+        )
+
+    w_away = pltpu.make_async_remote_copy(
+        src_ref=w_ref, dst_ref=wbuf.at[tp], send_sem=w_sem.at[1], recv_sem=w_sem.at[2],
+        device_id=target(sp, tp_count - 1 - tp), device_id_type=pl.DeviceIdType.MESH,
+    )
+
+    pairs = G // 2
+
+    def send(m):
+        for d in (2 * m, 2 * m + 1):
+
+            @pl.when(has_next)
+            def _():
+                copy_x(d).start()
+
+            @pl.when(d != me)
+            def _():
+                copy_kv(d).start()
+                copy_q(d).start()
+
+    for i in range(pairs):
+        m = lax.rem(me // 2 + i + 1, pairs)
+        cols = pl.ds(pl.multiple_of(m * LANES, LANES), LANES)
         tq = turn(q_ref, cols)
         tk = turn(k_ref, cols)
         tv = v_ref[:, cols]
@@ -123,55 +166,17 @@
             vs = sw(tv[e * BACK : (e + 1) * BACK])
             kvs[2 * m, e] = jnp.where(low, ks, pltpu.roll(vs, HD, 1)).astype(BF16)
             kvs[2 * m + 1, e] = jnp.where(low, pltpu.roll(ks, HD, 1), vs).astype(BF16)
-
-    pl.semaphore_wait(
-        barrier, seats - 1 + jnp.where(has_prev, G, 0) + jnp.where(has_next, G, 0)
-    )
-
-    own0 = G * halves
-
-    def copy_kv(dest):
-        return pltpu.make_async_remote_copy(
-            src_ref=kvs.at[dest], dst_ref=kv.at[pl.ds(own0 + halves * me, halves)],
-            send_sem=s_kv.at[dest], recv_sem=r_kv.at[me],
-            device_id=target(base + dest, tp), device_id_type=pl.DeviceIdType.MESH,
-        )
-
-    def copy_q(dest):
-        return pltpu.make_async_remote_copy(
-            src_ref=qs.at[dest], dst_ref=qr.at[me],
-            send_sem=s_q.at[dest], recv_sem=r_q.at[me],
-            device_id=target(base + dest, tp), device_id_type=pl.DeviceIdType.MESH,
-        )
-
-    def copy_x(dest):
-        return pltpu.make_async_remote_copy(
-            src_ref=kvs.at[dest], dst_ref=kv.at[pl.ds(halves * me, halves)],
-            send_sem=s_x.at[dest], recv_sem=r_x.at[me],
-            device_id=target(base + G + dest, tp), device_id_type=pl.DeviceIdType.MESH,
-        )
-
-    w_away = pltpu.make_async_remote_copy(
-        src_ref=w_ref, dst_ref=wbuf.at[tp], send_sem=w_sem.at[1], recv_sem=w_sem.at[2],
-        device_id=target(sp, tp_count - 1 - tp), device_id_type=pl.DeviceIdType.MESH,
-    )
-
-    for o in range(1, G):
-        copy_kv(lax.rem(me + o, G)).start()
-        copy_q(lax.rem(me + o, G)).start()
-
-    @pl.when(has_next)
-    def _():
-        for o in range(G):
-            copy_x(lax.rem(me + o, G)).start()
-
+        if i == 0:
+            pl.semaphore_wait(
+                barrier, seats - 1 + jnp.where(has_prev, G, 0) + jnp.where(has_next, G, 0)
+            )
+        else:
+            send(lax.rem(me // 2 + i, pairs))
+    send(lax.rem(me // 2 + pairs, pairs))
     w_away.start()
 
     row = iota((BACK, 2 * BACK), 0)
     col = iota((BACK, 2 * BACK), 1)
-    old = col < BACK
-    missing = jnp.logical_and(old, group == 0)
-
     def stride4(n):
         w = n & 31
         return ((n >> 5) << 5) + ((w & 7) << 2) + (w >> 3)
@@ -184,16 +189,10 @@
     b16 = masked(row + BACK - col)
     bias[0] = b1
     bias[1] = b4
-    bias[2] = jnp.where(missing, FAR, b1)
-    bias[3] = jnp.where(missing, FAR, b4)
-    bias[4] = jnp.where(missing, FAR, b16)
+    bias[2] = b16
 
     acc[...] = jnp.zeros_like(acc)
     top[...] = jnp.full_like(top, FAR)
-
-    @pl.when(jnp.logical_not(has_prev))
-    def _():
-        kv[:own0] = jnp.zeros((own0, BACK, LANES), BF16)
 
     kv[pl.ds(own0 + halves * me, halves)] = kvs[me]
     qr[me] = qs[me]
@@ -224,15 +223,17 @@
         ).wait_recv()
         ready(s)
 
-    low_keys = iota((2 * BACK, LANES), 1) < HD
-
     def attend(q, keys, b, o_old, t_old):
         s = lax.dot_general(q, keys, NT, preferred_element_type=F32) + b
         t_new = jnp.maximum(t_old, jnp.max(s, axis=1, keepdims=True))
         p = jnp.concatenate(
-            [jnp.exp(s[:, :BACK] - t_new), jnp.exp(s[:, BACK:] - t_new)], axis=1
-        ).astype(BF16)
-        ones = jnp.where(low_keys, jnp.ones_like(keys), keys)
+            [
+                jnp.exp(s[:, c : c + BACK] - t_new).astype(BF16)
+                for c in range(0, keys.shape[0], BACK)
+            ],
+            axis=1,
+        )
+        ones = jnp.where(iota(keys.shape, 1) < HD, jnp.ones_like(keys), keys)
         o = jnp.dot(p, ones, preferred_element_type=F32)
         return o_old * jnp.exp(t_old - t_new) + o, t_new
 
@@ -248,26 +249,33 @@
             acc[where] = o
             top[where] = t
 
-    def tile1(h, b):
-        return (
-            q2[h], kv[pl.ds(own0 - 1 + h, 2)].reshape(2 * BACK, LANES), bias[b], (h,),
-        )
-
-    def tile4(quarter, r, b):
+    mine = slice(BACK, 2 * BACK)
+    prior = slice(0, BACK)
+
+    def tile1(h, part):
+        keys = {None: pl.ds(own0 - 1 + h, 2), "own": own0 + h, "prior": own0 - 1 + h}[part]
+        cols = {None: slice(None), "own": mine, "prior": prior}[part]
+        return q2[h], kv[keys].reshape(-1, LANES), bias[0, :, cols], (h,)
+
+    def tile4(quarter, r, part):
         rows = pl.ds(r * 32, 32)
+        at = own0 + 4 * quarter
+        keys = {None: slice(at - 4, at + 4), "own": slice(at, at + 4), "prior": slice(at - 4, at)}[part]
+        cols = {None: slice(None), "own": mine, "prior": prior}[part]
         return (
             q2[4 * quarter : 4 * quarter + 4, rows, :].reshape(BACK, LANES),
-            kv[own0 + 4 * quarter - 4 : own0 + 4 * quarter + 4, rows, :].reshape(2 * BACK, LANES),
-            bias[b],
+            kv[keys, rows, :].reshape(-1, LANES),
+            bias[1, :, cols],
             (slice(4 * quarter, 4 * quarter + 4), rows, slice(None)),
         )
 
-    def tile16(r):
+    def tile16(r, part):
         rows = pl.ds(r * 8, 8)
+        keys = {"own": slice(own0, 2 * own0), "prior": slice(0, own0)}[part]
         return (
             q2f[:, rows, :].reshape(BACK, LANES).astype(BF16),
-            kvf[:, rows, :].reshape(2 * BACK, LANES).astype(BF16),
-            bias[4],
+            kvf[keys, rows, :].reshape(BACK, LANES).astype(BF16),
+            bias[2, :, {"own": mine, "prior": prior}[part]],
             (slice(None), rows, slice(None)),
         )
 
@@ -275,33 +283,41 @@
 
     @pl.loop(0, (nq - 1) // 3)
     def _(i):
-        run([tile1(1 + 3 * i + n, 0) for n in range(3)])
+        run([tile1(1 + 3 * i + n, None) for n in range(3)])
+
+    run([tile1(0, "own")])
 
     @pl.loop(0, 4)
     def _(r):
-        run([tile4(n, r, 1) for n in range(1, nq // 4)])
+        run([tile4(n, r, None) for n in range(1, nq // 4)])
+
+    run([tile4(0, r, "own") for r in range(4)])
+
+    @pl.loop(0, 4)
+    def _(i):
+        run([tile16(4 * i + n, "own") for n in range(4)])
+
+    def arrive(s):
+        pltpu.make_async_remote_copy(
+            src_ref=kvs.at[s], dst_ref=kv.at[pl.ds(halves * s, halves)],
+            send_sem=s_x.at[s], recv_sem=r_x.at[s],
+            device_id=target(base - G + s, tp), device_id_type=pl.DeviceIdType.MESH,
+        ).wait_recv()
+        at = pl.ds(halves * s, halves)
+        kvf[at] = kv[at].astype(F32)
 
     @pl.when(has_prev)
     def _():
-        for o in range(G):
-            s = lax.rem(me - o + G, G)
-            pltpu.make_async_remote_copy(
-                src_ref=kvs.at[s], dst_ref=kv.at[pl.ds(halves * s, halves)],
-                send_sem=s_x.at[s], recv_sem=r_x.at[s],
-                device_id=target(base - G + s, tp), device_id_type=pl.DeviceIdType.MESH,
-            ).wait_recv()
-
-    @pl.loop(0, G)
-    def _(i):
-        at = pl.ds(2 * i, 2)
-        kvf[at] = kv[at].astype(F32)
-
-    run([tile1(0, 2)])
-    run([tile4(0, r, 3) for r in range(4)])
-
-    @pl.loop(0, 4)
-    def _(i):
-        run([tile16(4 * i + n) for n in range(4)])
+        for s in range(G - 4 // halves, G):
+            arrive(s)
+        run([tile1(0, "prior")])
+        run([tile4(0, r, "prior") for r in range(4)])
+        for s in range(G - 4 // halves):
+            arrive(s)
+
+        @pl.loop(0, 4)
+        def _(i):
+            run([tile16(4 * i + n, "prior") for n in range(4)])
 
     @pl.loop(0, nq)
     def _(h):
@@ -410,7 +426,7 @@
             pltpu.VMEM((G * halves, BACK, LANES), F32),
             pltpu.VMEM((G * halves, BACK, LANES), F32),
             pltpu.VMEM((G * halves, BACK, LANES), F32),
-            pltpu.VMEM((5, BACK, 2 * BACK), F32),
+            pltpu.VMEM((3, BACK, 2 * BACK), F32),
             pltpu.VMEM((tp_count,) + out_weight.shape, BF16),
             pltpu.VMEM((seats, HD, LANES), BF16),
             pltpu.VMEM((seats, HD, LANES), BF16),

time: 45.3 us -> 56.5 us (1.25)
  Pallas kernels: 42.7 us -> 54.4 us
    pallas_call x1, Pallas kernels: 42.7 us -> 54.4 us  [per_device(): pl.pallas_call(functools.partial(kernel, G, ngroups, tp_count), out_shape...]
where the time goes in v3:
time: 56.5 us; the launch traced here: 56.3 us
  Pallas kernels  54.4 us (96%)
  local copies, waits for them, and re-layouts  1.88 us (3%)
    pallas_call x1, Pallas kernels, per_device(): pl.pallas_call(functools.partial(kernel, G, ngroups, tp_count), out_shape...  54.4 us
    unnamed x1, local copies, waits for them, and re-layouts  1.88 us

profile of v3, /device:TPU:17, one launch (start us, length us, event | category | flops | bytes accessed | tf_op | source)
XLA Modules:
  0.0 56.3 jit_solution(12718135728908408404)
XLA Ops:
  0.0 54.4 %shard_map.73 = bf16[128,2048]{1,0:T(8,128)(2,1)} custom-call(bf16[256,512]{1,0:T(8,128)(2,1)} %q_hbm.1, bf16[256,512]{1,0:T(8,128)(2,1)} %k_hbm.1, bf16[256,512]{1,0:T(8,128)(2,1)} %v_hbm.1, f32[256,128]{1,0:T(8,128)} %constant.6.clone.cosb_hbm, f32[256,128]{1,0:T(8,128)} %constant.7.clone.sinb_hbm, f32[8,128]{1,0:T(8,128)} %constant.8.clone.inv_hbm, ...), custom_call_target="tpu_custom_call" | custom-call | tf_op jit(solution)/shard_map/pallas_call | solution.py:408
  54.4 1.9 %copy.9 = bf16[128,2048]{1,0:T(8,128)(2,1)} copy(bf16[128,2048]{1,0:T(8,128)(2,1)} %shard_map.73) | data formatting | bytes 1048576

commit v4 on v2

--- a/solution.py
+++ b/solution.py
@@ -156,14 +156,20 @@
         device_id=target(sp, tp_count - 1 - tp), device_id_type=pl.DeviceIdType.MESH,
     )
 
-    for o in range(1, G):
-        copy_kv(lax.rem(me + o, G)).start()
-        copy_q(lax.rem(me + o, G)).start()
+    bits = [1 << n for n in range(G.bit_length() - 1)]
+    far = sorted(range(1, G), key=lambda o: -o.bit_count())
+
+    def mate(o):
+        return sum((((me // b + o // b) % 2) * b for b in bits), 0)
+
+    for o in far:
+        copy_kv(mate(o)).start()
+        copy_q(mate(o)).start()
 
     @pl.when(has_next)
     def _():
         for o in range(G):
-            copy_x(lax.rem(me + o, G)).start()
+            copy_x(mate(o)).start()
 
     w_away.start()
 
@@ -316,8 +322,10 @@
             device_id_type=pl.DeviceIdType.MESH,
         )
 
-    for o in range(1, seats):
-        copy_ret(lax.rem(seat + o, seats)).start()
+    for o in far + [0]:
+        copy_ret(mate(o) * tp_count + tp_count - 1 - tp).start()
+        if o:
+            copy_ret(mate(o) * tp_count + tp).start()
     rr[head] = rs[seat]
 
     for o in range(1, G):
@@ -379,6 +387,7 @@
     halves = tok // BACK
     ngroups = sp_count // G
     assert tok == 2 * BACK and tp_count == 2 and sp_count % G == 0
+    assert G & (G - 1) == 0
     assert G * tok == 16 * BACK
     inverse = np.power(THETA, -np.arange(HD // 2) / (HD // 2))
     inverse = np.tile(inverse, LANES // (HD // 2))[None, :]

time: 45.3 us -> 43.7 us (0.965)
  Pallas kernels: 42.7 us -> 41.4 us
    pallas_call x1, Pallas kernels: 42.7 us -> 41.4 us  [per_device(): pl.pallas_call(functools.partial(kernel, G, ngroups, tp_count), out_shape...]
where the time goes in v4:
time: 43.7 us; the launch traced here: 43.3 us
  Pallas kernels  41.4 us (95%)
  local copies, waits for them, and re-layouts  1.88 us (4%)
    pallas_call x1, Pallas kernels, per_device(): pl.pallas_call(functools.partial(kernel, G, ngroups, tp_count), out_shape...  41.4 us
    unnamed x1, local copies, waits for them, and re-layouts  1.88 us

profile of v4, /device:TPU:17, one launch (start us, length us, event | category | flops | bytes accessed | tf_op | source)
XLA Modules:
  0.0 43.3 jit_solution(5071333325462541626)
XLA Ops:
  0.0 41.4 %shard_map.73 = bf16[128,2048]{1,0:T(8,128)(2,1)} custom-call(bf16[256,512]{1,0:T(8,128)(2,1)} %q_hbm.1, bf16[256,512]{1,0:T(8,128)(2,1)} %k_hbm.1, bf16[256,512]{1,0:T(8,128)(2,1)} %v_hbm.1, f32[256,128]{1,0:T(8,128)} %constant.6.clone.cosb_hbm, f32[256,128]{1,0:T(8,128)} %constant.7.clone.sinb_hbm, f32[8,128]{1,0:T(8,128)} %constant.8.clone.inv_hbm, ...), custom_call_target="tpu_custom_call" | custom-call | tf_op jit(solution)/shard_map/pallas_call | solution.py:401
  41.4 1.9 %copy.9 = bf16[128,2048]{1,0:T(8,128)(2,1)} copy(bf16[128,2048]{1,0:T(8,128)(2,1)} %shard_map.73) | data formatting | bytes 1048576

commit v5 on v4

--- a/solution.py
+++ b/solution.py
@@ -287,23 +287,26 @@
     def _(r):
         run([tile4(n, r, 1) for n in range(1, nq // 4)])
 
-    @pl.when(has_prev)
-    def _():
-        for o in range(G):
-            s = lax.rem(me - o + G, G)
-            pltpu.make_async_remote_copy(
-                src_ref=kvs.at[s], dst_ref=kv.at[pl.ds(halves * s, halves)],
-                send_sem=s_x.at[s], recv_sem=r_x.at[s],
-                device_id=target(base - G + s, tp), device_id_type=pl.DeviceIdType.MESH,
-            ).wait_recv()
-
-    @pl.loop(0, G)
-    def _(i):
-        at = pl.ds(2 * i, 2)
-        kvf[at] = kv[at].astype(F32)
-
+    def arrive(sources):
+        @pl.when(has_prev)
+        def _():
+            for s in sources:
+                at = pl.ds(halves * s, halves)
+                pltpu.make_async_remote_copy(
+                    src_ref=kvs.at[s], dst_ref=kv.at[at], send_sem=s_x.at[s], recv_sem=r_x.at[s],
+                    device_id=target(base - G + s, tp), device_id_type=pl.DeviceIdType.MESH,
+                ).wait_recv()
+                kvf[at] = kv[at].astype(F32)
+
+    @pl.when(jnp.logical_not(has_prev))
+    def _():
+        kvf[:own0] = jnp.zeros((own0, BACK, LANES), F32)
+
+    arrive(range(G - 4 // halves, G))
     run([tile1(0, 2)])
     run([tile4(0, r, 3) for r in range(4)])
+
+    arrive(range(G - 4 // halves))
 
     @pl.loop(0, 4)
     def _(i):

time: 43.7 us -> 43.2 us (0.989)
  no operation moved by 1% of the time
where the time goes in v5:
time: 43.2 us; the launch traced here: 43 us
  Pallas kernels  41.1 us (95%)
  local copies, waits for them, and re-layouts  1.88 us (4%)
    pallas_call x1, Pallas kernels, per_device(): pl.pallas_call(functools.partial(kernel, G, ngroups, tp_count), out_shape...  41.1 us
    unnamed x1, local copies, waits for them, and re-layouts  1.88 us

profile of v5, /device:TPU:17, one launch (start us, length us, event | category | flops | bytes accessed | tf_op | source)
XLA Modules:
  0.0 43.0 jit_solution(5179866640697724688)
XLA Ops:
  0.0 41.1 %shard_map.73 = bf16[128,2048]{1,0:T(8,128)(2,1)} custom-call(bf16[256,512]{1,0:T(8,128)(2,1)} %q_hbm.1, bf16[256,512]{1,0:T(8,128)(2,1)} %k_hbm.1, bf16[256,512]{1,0:T(8,128)(2,1)} %v_hbm.1, f32[256,128]{1,0:T(8,128)} %constant.6.clone.cosb_hbm, f32[256,128]{1,0:T(8,128)} %constant.7.clone.sinb_hbm, f32[8,128]{1,0:T(8,128)} %constant.8.clone.inv_hbm, ...), custom_call_target="tpu_custom_call" | custom-call | tf_op jit(solution)/shard_map/pallas_call | solution.py:404
  41.1 1.9 %copy.9 = bf16[128,2048]{1,0:T(8,128)(2,1)} copy(bf16[128,2048]{1,0:T(8,128)(2,1)} %shard_map.73) | data formatting | bytes 1048576
